TPU v7x, 256 devices: a whole 4x4x8 slice. The times are simulated.
256 devices in a mesh: ep: 16 (over y, x), tp: 16 (over z, core).
Axes of the slice: x: 4, y: 4, z: 8, core: 2. Of those that a mesh axis runs over, the one named last changes fastest.
Arguments:
- stream: bfloat16 [131072, 1024], P(('ep', 'tp')), may hold values from -6 to 6
- norm_gain: float32 [1024], replicated, may hold values from 0.5 to 1.5
- gate_rows: bfloat16 [16, 1024, 1024], P('ep', 'tp'), may hold values from -0.1875 to 0.1875
- up_rows: bfloat16 [16, 1024, 1024], P('ep', 'tp'), may hold values from -0.1875 to 0.1875
- down_rows: bfloat16 [16, 1024, 1024], P('ep', 'tp'), may hold values from -0.1875 to 0.1875
- chosen: int32 [16, 16384], P('ep'), may hold values from 0 to 131071, as said below
- affinity: float32 [16, 16384], P('ep'), may hold values from 0.2 to 1
Outputs:
- mixed_out: bfloat16 [131072, 1024], P(('ep', 'tp'))
Inputs may be any that keep to these rules, and one draw needn't show every extreme that they name: Each row of chosen names 16384 different token numbers in increasing order. Among the 512 consecutive token numbers of any one device, an expert reads at most 128, and for every expert some device holds exactly 128 of its tokens.
All inputs are finite; a program needn't handle non-finite values.
Results may differ from a plain program's by a relative error of at most 0.008.
Values may be sent and summed in bfloat16 or wider, within the bound.
No kernel may reach another device: no remote copies, remote signals or barrier semaphores. Data moves between devices by JAX's collectives and lax.ppermute only.
A program may use at most 64 MiB of HBM per device.

v0:
```python
import functools

import jax
import jax.numpy as jnp
from jax import lax
from jax.experimental import pallas as pl
from jax.experimental.pallas import tpu as pltpu
from jax.sharding import PartitionSpec as P

epsilon = 1e-06
SIDE = 4
SMEM = pl.BlockSpec(memory_space=pltpu.SMEM)
VMEM = pl.BlockSpec(memory_space=pltpu.VMEM)


def wrap(value):
    return lax.rem(value + SIDE, SIDE)


def windows_kernel(block, slots, bounds_ref, list_ref, affinity_ref, rows_ref, weights_ref):
    listed = list_ref[...]
    lines = listed.shape[0]
    lane = lax.broadcasted_iota(jnp.int32, (1, slots), 1)
    for j in range(weights_ref.shape[0]):
        y, x = divmod(j, SIDE)
        bound = bounds_ref[j]
        start = jnp.sum((listed < bound).astype(jnp.int32))
        line, shift = start // slots, start % slots
        first = jnp.minimum(line, lines - 1)
        second = jnp.minimum(line + 1, lines - 1)
        back = lax.rem(slots - shift, slots)

        def window(ref):
            low = pltpu.roll(ref[pl.ds(first, 1), :], back, 1)
            high = pltpu.roll(ref[pl.ds(second, 1), :], back, 1)
            return jnp.where(lane < slots - shift, low, high)

        rows = window(list_ref) - bound
        rows = jnp.where((rows >= 0) & (rows < block), rows, -1)
        for t in range(SIDE):
            rows_ref[y * SIDE + (x + t) % SIDE, t : t + 1, :] = rows
            rows_ref[(y + t) % SIDE * SIDE + x, SIDE + t : SIDE + t + 1, :] = rows
        weights_ref[j : j + 1, :] = window(affinity_ref)


def windows(bounds, listed, affinity, block, slots):
    count = bounds.shape[0]
    return pl.pallas_call(
        functools.partial(windows_kernel, block, slots),
        in_specs=[SMEM, VMEM, VMEM],
        out_shape=(
            jax.ShapeDtypeStruct((count, 2 * SIDE, slots), jnp.int32),
            jax.ShapeDtypeStruct((count, slots), jnp.float32),
        ),
        cost_estimate=pl.CostEstimate(flops=8_000_000, bytes_accessed=150_000, transcendentals=0),
        name="windows",
    )(bounds, listed.reshape(-1, slots), affinity.reshape(-1, slots))


def prepare_kernel(stream_ref, gain_ref, gate_ref, up_ref, down_ref, low_ref, high_ref, piece_ref):
    values = stream_ref[...].astype(jnp.float32)
    inverse = lax.rsqrt(jnp.mean(values * values, axis=-1, keepdims=True) + epsilon)
    normed = (values * inverse * gain_ref[...]).astype(jnp.bfloat16)
    half = low_ref.shape[1]
    low_ref[...] = normed[:, :half]
    high_ref[...] = normed[:, half:]

    @pl.when(pl.program_id(0) == 0)
    def _():
        piece_ref[0:1] = gate_ref[...]
        piece_ref[1:2] = up_ref[...]
        piece_ref[2:3] = down_ref[...]


def prepare(stream, norm_gain, parts):
    rows, features = stream.shape
    step, half = rows // 2, features // 2
    part = pl.BlockSpec(parts[0].shape, lambda i: (0, 0, 0))
    piece = (3, *parts[0].shape[1:])
    return pl.pallas_call(
        prepare_kernel,
        grid=(2,),
        in_specs=[
            pl.BlockSpec((step, features), lambda i: (i, 0)),
            pl.BlockSpec((1, features), lambda i: (0, 0)),
            part,
            part,
            part,
        ],
        out_specs=(
            pl.BlockSpec((step, half), lambda i: (i, 0)),
            pl.BlockSpec((step, half), lambda i: (i, 0)),
            pl.BlockSpec(piece, lambda i: (0, 0, 0)),
        ),
        out_shape=(
            jax.ShapeDtypeStruct((rows, half), jnp.bfloat16),
            jax.ShapeDtypeStruct((rows, half), jnp.bfloat16),
            jax.ShapeDtypeStruct(piece, jnp.bfloat16),
        ),
        cost_estimate=pl.CostEstimate(flops=3_000_000, bytes_accessed=3 << 20, transcendentals=512),
        name="prepare",
    )(stream, norm_gain.reshape(1, features), *parts)


def pick_kernel(along_y, place_ref, rows_ref, *refs):
    sources, outs = refs[:SIDE], refs[SIDE:]
    y, x = place_ref[0], place_ref[1]
    tokens, slots = sources[0].shape[0], rows_ref.shape[2]
    token = lax.broadcasted_iota(jnp.int32, (slots, tokens), 1).astype(jnp.float32)
    columns = []
    for d in range(SIDE):
        e = wrap(y + d) * SIDE + x if along_y else y * SIDE + wrap(x + d)
        columns.append(rows_ref[e].astype(jnp.float32).T)
    for t in range(SIDE):
        k = t if along_y else SIDE + t
        chosen = jnp.concatenate(
            [jnp.where(column[:, k : k + 1] == token, 1.0, 0.0).astype(jnp.bfloat16) for column in columns]
        )
        rows = jnp.dot(chosen, sources[t][...], preferred_element_type=jnp.float32).astype(jnp.bfloat16)
        for d in range(SIDE):
            outs[d][t * slots : (t + 1) * slots, :] = rows[d * slots : (d + 1) * slots, :]


def pick(along_y, place, rows, sources):
    tokens, half = sources[0].shape
    slots = rows.shape[2]
    return pl.pallas_call(
        functools.partial(pick_kernel, along_y),
        in_specs=[SMEM] + [VMEM] * (1 + SIDE),
        out_shape=[jax.ShapeDtypeStruct((SIDE * slots, half), jnp.bfloat16)] * SIDE,
        cost_estimate=pl.CostEstimate(
            flops=2 * SIDE * SIDE * slots * tokens * half, bytes_accessed=4 << 20, transcendentals=0
        ),
        compiler_params=pltpu.CompilerParams(vmem_limit_bytes=12 << 20),
        name="pick_y" if along_y else "pick_x",
    )(place, rows, *sources)


def assemble_kernel(*refs):
    pieces, outs = refs[:-3], refs[-3:]
    width = pieces[0].shape[1]
    for k, piece in enumerate(pieces):
        for j, out in enumerate(outs):
            out[k * width : (k + 1) * width, :] = piece[j]


def assemble(pieces):
    shape = jax.ShapeDtypeStruct((len(pieces) * pieces[0].shape[1], pieces[0].shape[2]), jnp.bfloat16)
    return pl.pallas_call(
        assemble_kernel,
        in_specs=[VMEM] * len(pieces),
        out_shape=[shape] * 3,
        cost_estimate=pl.CostEstimate(flops=1_000_000, bytes_accessed=12 << 20, transcendentals=0),
        compiler_params=pltpu.CompilerParams(vmem_limit_bytes=16 << 20),
        name="assemble",
    )(*pieces)


def expert_kernel(place_ref, weights_ref, gate_ref, up_ref, down_ref, *refs):
    low, high = refs[:SIDE], refs[SIDE : 2 * SIDE]
    out_ref, inputs_ref = refs[2 * SIDE :]
    y, x = place_ref[0], place_ref[1]
    slots, half = out_ref.shape[1], low[0].shape[1]
    a = pl.program_id(0)
    for k in range(SIDE):

        @pl.when(a == k)
        def _():
            inputs_ref[:, :half] = low[k][...]

        inputs_ref[k * slots : (k + 1) * slots, half:] = high[k][pl.ds(pl.multiple_of(a * slots, slots), slots), :]
    last = (((1,), (1,)), ((), ()))
    inputs = inputs_ref[...]
    units = gate_ref.shape[0]
    width = units // 4
    hidden = []
    for f in range(0, units, width):
        gate_sum = lax.dot_general(inputs, gate_ref[f : f + width, :], last, preferred_element_type=jnp.float32)
        up_sum = lax.dot_general(inputs, up_ref[f : f + width, :], last, preferred_element_type=jnp.float32)
        hidden.append((gate_sum / (1.0 + jnp.exp(-gate_sum)) * up_sum).astype(jnp.bfloat16))
    result = jnp.dot(jnp.concatenate(hidden, 1), down_ref[...], preferred_element_type=jnp.float32)
    for b in range(SIDE):
        back = wrap(x - b)
        line = weights_ref[pl.ds(wrap(y - a) * SIDE + back, 1), :]
        column = jnp.broadcast_to(line, (slots, slots)).T[:, :1]
        out_ref[back] = (result[b * slots : (b + 1) * slots] * column).astype(jnp.bfloat16)


def expert(place, weights, low, high, gate, up, down):
    slots, half = weights.shape[1], low[0].shape[1]
    features, units = 2 * half, gate.shape[0]
    total = SIDE * SIDE * slots
    whole = pl.BlockSpec(memory_space=pltpu.VMEM)
    return pl.pallas_call(
        expert_kernel,
        grid_spec=pltpu.PrefetchScalarGridSpec(
            num_scalar_prefetch=1,
            grid=(SIDE,),
            in_specs=[whole] * (4 + len(low) + len(high)),
            out_specs=pl.BlockSpec((SIDE, slots, features), lambda a, place_ref: (wrap(place_ref[0] - a), 0, 0)),
            scratch_shapes=[pltpu.VMEM((SIDE * slots, features), jnp.bfloat16)],
        ),
        out_shape=jax.ShapeDtypeStruct((SIDE * SIDE, slots, features), jnp.bfloat16),
        cost_estimate=pl.CostEstimate(
            flops=6 * total * units * features,
            bytes_accessed=6 * units * features + 4 * total * features,
            transcendentals=2 * total * units,
        ),
        compiler_params=pltpu.CompilerParams(vmem_limit_bytes=36 << 20),
        name="expert",
    )(place, weights, gate, up, down, *low, *high)


def combine_kernel(rows_ref, returned_ref, out_ref, chosen_ref):
    @pl.when(pl.program_id(0) == 0)
    def _():
        count, _, slots = rows_ref.shape
        token = lax.broadcasted_iota(jnp.int32, (chosen_ref.shape[0], slots), 0)
        for e in range(count):
            chosen_ref[:, e * slots : (e + 1) * slots] = jnp.where(token == rows_ref[e, 0:1, :], 1.0, 0.0).astype(
                jnp.bfloat16
            )

    out_ref[...] = jnp.dot(chosen_ref[...], returned_ref[...], preferred_element_type=jnp.float32).astype(jnp.bfloat16)


def combine(rows, returned, tokens):
    total, features = returned.shape
    step = 256
    return pl.pallas_call(
        combine_kernel,
        grid=(features // step,),
        in_specs=[
            pl.BlockSpec(rows.shape, lambda i: (0, 0, 0)),
            pl.BlockSpec((total, step), lambda i: (0, i)),
        ],
        out_specs=pl.BlockSpec((tokens, step), lambda i: (0, i)),
        out_shape=jax.ShapeDtypeStruct((tokens, features), jnp.bfloat16),
        scratch_shapes=[pltpu.VMEM((tokens, total), jnp.bfloat16)],
        cost_estimate=pl.CostEstimate(
            flops=2 * total * tokens * features, bytes_accessed=2 * total * features, transcendentals=0
        ),
        compiler_params=pltpu.CompilerParams(vmem_limit_bytes=16 << 20),
        name="combine",
    )(rows, returned)


def over_plane(array, by_y, by_x):
    places = [(y, x) for y in range(SIDE) for x in range(SIDE)]
    return lax.ppermute(
        array, "ep", [(y * SIDE + x, (y + by_y) % SIDE * SIDE + (x + by_x) % SIDE) for y, x in places]
    )


def along_z(array, by, tp_count):
    chips = tp_count // 2
    return lax.ppermute(array, "tp", [(z * 2 + c, (z + by) % chips * 2 + c) for z in range(chips) for c in range(2)])


def other_core(array, tp_count):
    return lax.ppermute(array, "tp", [(j, j ^ 1) for j in range(tp_count)])


def layer(stream, norm_gain, gate_rows, up_rows, down_rows, chosen, affinity):
    ep_count = lax.axis_size("ep")
    tp_count = lax.axis_size("tp")
    block, features = stream.shape
    slots = 4 * block // ep_count
    ep_index = lax.axis_index("ep").astype(jnp.int32)
    place = jnp.stack([ep_index // SIDE, ep_index % SIDE])
    bounds = (jnp.arange(ep_count, dtype=jnp.int32) * tp_count + lax.axis_index("tp")) * block
    low, high, own = prepare(stream, norm_gain, (gate_rows, up_rows, down_rows))
    lows = [low] + [over_plane(low, 0, t) for t in range(1, SIDE)]
    highs = [high] + [over_plane(high, t, 0) for t in range(1, SIDE)]
    rows_there, weights = windows(bounds, chosen, affinity, block, slots)
    rows_here = lax.all_to_all(rows_there, "ep", split_axis=0, concat_axis=0, tiled=True)
    near = {by: along_z(own, by, tp_count) for by in (1, -1, 2, -2)}
    picked_low = pick(True, place, rows_here, lows)
    arrived_low = [picked_low[0]] + [over_plane(picked_low[d], d, 0) for d in range(1, SIDE)]
    picked_high = pick(False, place, rows_here, highs)
    arrived_high = [picked_high[0]] + [over_plane(picked_high[d], 0, d) for d in range(1, SIDE)]
    far = [along_z(near[2], 1, tp_count), along_z(near[-2], -1, tp_count), along_z(near[2], 2, tp_count)]
    held = [own, *near.values(), *far]
    pieces = held + [other_core(piece, tp_count) for piece in held]
    produced = expert(place, weights, arrived_low, arrived_high, *assemble(pieces))
    returned = lax.all_to_all(produced, "ep", split_axis=0, concat_axis=0, tiled=True)
    return combine(rows_here, returned.reshape(-1, features), block)


def solution(mesh):
    return jax.shard_map(
        layer,
        mesh=mesh,
        in_specs=(
            P(("ep", "tp"), None),
            P(),
            P("ep", "tp", None),
            P("ep", "tp", None),
            P("ep", "tp", None),
            P("ep", None),
            P("ep", None),
        ),
        out_specs=P(("ep", "tp"), None),
        check_vma=False,
    )
```

profile of v0, /device:TPU:1, one launch (start us, length us, event | category | flops | bytes accessed | tf_op | source)
XLA Modules:
  0.0 201.8 jit_solution(6953989833272391081)
XLA Ops:
  0.0 2.6 %prepare.1 = (bf16[512,512]{1,0:T(8,128)(2,1)}, bf16[512,512]{1,0:T(8,128)(2,1)}, bf16[3,64,1024]{2,1,0:T(8,128)(2,1)}) custom-call(bf16[512,1024]{1,0:T(8,128)(2,1)} %stream_ref.1, f32[1,1024]{1,0:T(1,128)} %bitcast.9, bf16[1,64,1024]{2,1,0:T(8,128)(2,1)} %gate_ref.1, bf16[1,64,1024]{2,1,0:T(8,128)(2,1)} %up_ref.1, bf16[1,64,1024]{2,1,0:T(8,128)(2,1)} %down_ref.1), custom_call_target="tpu_custom_call" | custom-call | flops 3000000 | bytes 3145728 | tf_op jit(solution)/shard_map/prepare/pallas_call | solution.py:80
  2.6 3.3 %collective-permute-start.7 = (bf16[3,64,1024]{2,1,0:T(8,128)(2,1)}, bf16[3,64,1024]{2,1,0:T(8,128)(2,1)S(1)}, u32[]{:S(2)}, u32[]{:S(2)}) collective-permute-start(bf16[3,64,1024]{2,1,0:T(8,128)(2,1)} %get-tuple-element.23.refs_0_), channel_id=1, source_target_pairs={{0,1},{1,0},{2,3},{3,2},{4,5},{5,4},{6,7},{7,6},{8,9},{9,8},{10,11... | collective-permute-start | bytes 1179656 | tf_op jit(solution)/shard_map/ppermute | solution.py:261
  5.9 4.3 %collective-permute-start.3 = (bf16[3,64,1024]{2,1,0:T(8,128)(2,1)}, bf16[3,64,1024]{2,1,0:T(8,128)(2,1)S(1)}, u32[]{:S(2)}, u32[]{:S(2)}) collective-permute-start(bf16[3,64,1024]{2,1,0:T(8,128)(2,1)} %get-tuple-element.23.refs_0_), channel_id=1, source_target_pairs={{0,12},{1,13},{2,14},{3,15},{4,0},{5,1},{6,2},{7,3},{8,4},{9,5},{1... | collective-permute-start | bytes 1179656 | tf_op jit(solution)/shard_map/ppermute | solution.py:257
  10.2 2.5 %collective-permute-start.17 = (bf16[512,512]{1,0:T(8,128)(2,1)}, bf16[512,512]{1,0:T(8,128)(2,1)S(1)}, u32[]{:S(2)}, u32[]{:S(2)}) collective-permute-start(bf16[512,512]{1,0:T(8,128)(2,1)} %get-tuple-element.27.refs_0_), channel_id=1, source_target_pairs={{0,48},{16,0},{32,16},{48,32},{64,112},{80,64},{96,80},{112,96},{1... | collective-permute-start | bytes 1572872 | tf_op jit(solution)/shard_map/ppermute | solution.py:250
  12.7 3.1 %collective-permute-start.1 = (bf16[3,64,1024]{2,1,0:T(8,128)(2,1)}, bf16[3,64,1024]{2,1,0:T(8,128)(2,1)S(1)}, u32[]{:S(2)}, u32[]{:S(2)}) collective-permute-start(bf16[3,64,1024]{2,1,0:T(8,128)(2,1)} %get-tuple-element.23.refs_0_), channel_id=1, source_target_pairs={{0,14},{1,15},{2,0},{3,1},{4,2},{5,3},{6,4},{7,5},{8,6},{9,7},{10,... | collective-permute-start | bytes 1179656 | tf_op jit(solution)/shard_map/ppermute | solution.py:257
  15.8 10.3 %collective-permute-done.3.refs_4_ = bf16[3,64,1024]{2,1,0:T(8,128)(2,1)S(1)} collective-permute-done((bf16[3,64,1024]{2,1,0:T(8,128)(2,1)}, bf16[3,64,1024]{2,1,0:T(8,128)(2,1)S(1)}, u32[]{:S(2)}, u32[]{:S(2)}) %collective-permute-start.3) | collective-permute-done | bytes 393248 | tf_op jit(solution)/shard_map/ppermute | solution.py:257
  26.2 3.4 %collective-permute-start.16 = (bf16[512,512]{1,0:T(8,128)(2,1)}, bf16[512,512]{1,0:T(8,128)(2,1)S(1)}, u32[]{:S(2)}, u32[]{:S(2)}) collective-permute-start(bf16[512,512]{1,0:T(8,128)(2,1)} %get-tuple-element.27.refs_0_), channel_id=1, source_target_pairs={{0,32},{16,48},{32,0},{48,16},{64,96},{80,112},{96,64},{112,80},{1... | collective-permute-start | bytes 1572872 | tf_op jit(solution)/shard_map/ppermute | solution.py:250
  29.9 7.0 %collective-permute-done.1.refs_2_ = bf16[3,64,1024]{2,1,0:T(8,128)(2,1)S(1)} collective-permute-done((bf16[3,64,1024]{2,1,0:T(8,128)(2,1)}, bf16[3,64,1024]{2,1,0:T(8,128)(2,1)S(1)}, u32[]{:S(2)}, u32[]{:S(2)}) %collective-permute-start.1) | collective-permute-done | bytes 393248 | tf_op jit(solution)/shard_map/ppermute | solution.py:257
  38.6 3.4 %collective-permute-done.refs_1_ = bf16[3,64,1024]{2,1,0:T(8,128)(2,1)S(1)} collective-permute-done((bf16[3,64,1024]{2,1,0:T(8,128)(2,1)}, bf16[3,64,1024]{2,1,0:T(8,128)(2,1)S(1)}, u32[]{:S(2)}, u32[]{:S(2)}) %collective-permute-start) | collective-permute-done | bytes 393248 | tf_op jit(solution)/shard_map/ppermute | solution.py:257
  42.0 2.9 %collective-permute-start.22 = (bf16[512,512]{1,0:T(8,128)(2,1)}, bf16[512,512]{1,0:T(8,128)(2,1)}, u32[]{:S(2)}, u32[]{:S(2)}) collective-permute-start(bf16[512,512]{1,0:T(8,128)(2,1)} %get-tuple-element.32.refs_0_), channel_id=1, source_target_pairs={{0,128},{16,144},{32,160},{48,176},{64,192},{80,208},{96,224},{112... | collective-permute-start | bytes 1572872 | tf_op jit(solution)/shard_map/ppermute | solution.py:250
  48.4 5.1 %collective-permute-done.15.refs_1_ = bf16[512,512]{1,0:T(8,128)(2,1)S(1)} collective-permute-done((bf16[512,512]{1,0:T(8,128)(2,1)}, bf16[512,512]{1,0:T(8,128)(2,1)S(1)}, u32[]{:S(2)}, u32[]{:S(2)}) %collective-permute-start.15) | collective-permute-done | bytes 524320 | tf_op jit(solution)/shard_map/ppermute | solution.py:250
  54.3 4.3 %collective-permute-start.5 = (bf16[3,64,1024]{2,1,0:T(8,128)(2,1)S(1)}, bf16[3,64,1024]{2,1,0:T(8,128)(2,1)S(1)}, u32[]{:S(2)}, u32[]{:S(2)}) collective-permute-start(bf16[3,64,1024]{2,1,0:T(8,128)(2,1)S(1)} %collective-permute-done.3.refs_4_), channel_id=1, source_target_pairs={{0,14},{1,15},{2,0},{3,1},{4,2},{5,3},{6,4},{7,5},{8,6},{9,7},{10,... | collective-permute-start | bytes 1179656 | tf_op jit(solution)/shard_map/ppermute | solution.py:257
  59.4 3.7 %collective-permute-start.10 = (bf16[3,64,1024]{2,1,0:T(8,128)(2,1)S(1)}, bf16[3,64,1024]{2,1,0:T(8,128)(2,1)S(1)}, u32[]{:S(2)}, u32[]{:S(2)}) collective-permute-start(bf16[3,64,1024]{2,1,0:T(8,128)(2,1)S(1)} %collective-permute-done.2.refs_3_), channel_id=1, source_target_pairs={{0,1},{1,0},{2,3},{3,2},{4,5},{5,4},{6,7},{7,6},{8,9},{9,8},{10,11... | collective-permute-start | bytes 1179656 | tf_op jit(solution)/shard_map/ppermute | solution.py:261
  63.1 5.8 %collective-permute-done.21.refs_1_ = bf16[512,512]{1,0:T(8,128)(2,1)} collective-permute-done((bf16[512,512]{1,0:T(8,128)(2,1)}, bf16[512,512]{1,0:T(8,128)(2,1)}, u32[]{:S(2)}, u32[]{:S(2)}) %collective-permute-start.21) | collective-permute-done | bytes 524320 | tf_op jit(solution)/shard_map/ppermute | solution.py:250
  70.0 2.6 %windows.1 = (s32[16,8,128]{2,1,0:T(8,128)}, f32[16,128]{1,0:T(8,128)}) custom-call(s32[16]{0:T(128)} %add_multiply_fusion.bounds_ref, s32[128,128]{1,0:T(8,128)} %bitcast.7, f32[128,128]{1,0:T(8,128)} %bitcast.8), custom_call_target="tpu_custom_call" | custom-call | flops 8000000 | bytes 150000 | tf_op jit(solution)/shard_map/windows/pallas_call | solution.py:48
  72.5 4.6 %all-to-all-start = ((s32[16,8,128]{2,1,0:T(8,128)}), s32[16,8,128]{2,1,0:T(8,128)}, u32[]{:S(2)}, u32[]{:S(2)}) async-start(s32[16,8,128]{2,1,0:T(8,128)} %get-tuple-element.21), calls=%async_computation | async-start | bytes 131072 | tf_op jit(solution)/shard_map/all_to_all | solution.py:276
  77.3 6.5 %all-to-all-done.rows_ref = s32[16,8,128]{2,1,0:T(8,128)} async-done(((s32[16,8,128]{2,1,0:T(8,128)}), s32[16,8,128]{2,1,0:T(8,128)}, u32[]{:S(2)}, u32[]{:S(2)}) %all-to-all-start) | async-done | bytes 65568 | tf_op jit(solution)/shard_map/all_to_all | solution.py:276
  93.4 2.8 %pick_x.1 = (bf16[512,512]{1,0:T(8,128)(2,1)S(1)}, bf16[512,512]{1,0:T(8,128)(2,1)S(1)}, bf16[512,512]{1,0:T(8,128)(2,1)S(1)}, bf16[512,512]{1,0:T(8,128)(2,1)S(1)}) custom-call(s32[2]{0:T(128)S(1)} %pad_add_fusion.place_ref, s32[16,8,128]{2,1,0:T(8,128)} %all-to-all-done.rows_ref, bf16[512,512]{1,0:T(8,128)(2,1)S(1)} %copy-done.1, ...), custom_call_target="tpu_custom_call" | custom-call | flops 1073741824 | bytes 4194304 | tf_op jit(solution)/shard_map/pick_x/pallas_call | solution.py:127
  97.7 6.7 %collective-permute-done.18.refs_1_ = bf16[512,512]{1,0:T(8,128)(2,1)S(1)} collective-permute-done((bf16[512,512]{1,0:T(8,128)(2,1)S(1)}, bf16[512,512]{1,0:T(8,128)(2,1)S(1)}, u32[]{:S(2)}, u32[]{:S(2)}) %collective-permute-start.18) | collective-permute-done | bytes 524320 | tf_op jit(solution)/shard_map/ppermute | solution.py:250
  109.6 4.8 %collective-permute-done.19.refs_2_ = bf16[512,512]{1,0:T(8,128)(2,1)S(1)} collective-permute-done((bf16[512,512]{1,0:T(8,128)(2,1)S(1)}, bf16[512,512]{1,0:T(8,128)(2,1)S(1)}, u32[]{:S(2)}, u32[]{:S(2)}) %collective-permute-start.19) | collective-permute-done | bytes 524320 | tf_op jit(solution)/shard_map/ppermute | solution.py:250
  114.3 3.6 %collective-permute-done.20.refs_3_ = bf16[512,512]{1,0:T(8,128)(2,1)S(1)} collective-permute-done((bf16[512,512]{1,0:T(8,128)(2,1)S(1)}, bf16[512,512]{1,0:T(8,128)(2,1)S(1)}, u32[]{:S(2)}, u32[]{:S(2)}) %collective-permute-start.20) | collective-permute-done | bytes 524320 | tf_op jit(solution)/shard_map/ppermute | solution.py:250
  119.9 14.8 %expert.1 = bf16[16,128,1024]{2,1,0:T(8,128)(2,1)S(1)} custom-call(s32[2]{0:T(128)S(1)} %pad_add_fusion.place_ref, f32[16,128]{1,0:T(8,128)S(1)} %copy-done.11, bf16[1024,1024]{1,0:T(8,128)(2,1)S(1)} %get-tuple-element.24.gate_ref, bf16[1024,1024]{1,0:T(8,128)(2,1)S(1)} %get-tuple-element.25.up_ref, bf16[1024,1024]{1,0:T(8,128)(2,1)S(1)} %get-tuple-element.26.down_ref, ...), custom_call_target="tpu_custom_call" | custom-call | flops 12884901888 | bytes 14680064 | tf_op jit(solution)/shard_map/expert/pallas_call | solution.py:194
  134.7 61.6 %all_to_all.10 = bf16[16,128,1024]{2,1,0:T(8,128)(2,1)S(1)} all-to-all(bf16[16,128,1024]{2,1,0:T(8,128)(2,1)S(1)} %expert.1), channel_id=1, replica_groups=mesh['ep'=16,'tp'=16] {'ep'}, dimensions={0} | all-to-all | bytes 8388608 | tf_op jit(solution)/shard_map/all_to_all | solution.py:286
  196.4 5.5 %combine.1 = bf16[512,1024]{1,0:T(8,128)(2,1)} custom-call(s32[16,8,128]{2,1,0:T(8,128)} %all-to-all-done.rows_ref, bf16[2048,1024]{1,0:T(8,128)(2,1)S(1)} %bitcast.6), custom_call_target="tpu_custom_call" | custom-call | flops 2147483648 | bytes 4194304 | tf_op jit(solution)/shard_map/combine/pallas_call | solution.py:230
  (66 shorter events, 26.5 us)
Async XLA Ops:
  2.6 13.2 %collective-permute-start.7 = (bf16[3,64,1024]{2,1,0:T(8,128)(2,1)}, bf16[3,64,1024]{2,1,0:T(8,128)(2,1)S(1)}, u32[]{:S(2)}, u32[]{:S(2)}) collective-permute-start(bf16[3,64,1024]{2,1,0:T(8,128)(2,1)} %get-tuple-element.23.refs_0_), channel_id=1, source_target_pairs={{0,1},{1,0},{2,3},{3,2},{4,5},{5,4},{6,7},{7,6},{8,9},{9,8},{10,11... | collective-permute-start | bytes 1179656 | tf_op jit(solution)/shard_map/ppermute | solution.py:261
  5.9 20.3 %collective-permute-start.3 = (bf16[3,64,1024]{2,1,0:T(8,128)(2,1)}, bf16[3,64,1024]{2,1,0:T(8,128)(2,1)S(1)}, u32[]{:S(2)}, u32[]{:S(2)}) collective-permute-start(bf16[3,64,1024]{2,1,0:T(8,128)(2,1)} %get-tuple-element.23.refs_0_), channel_id=1, source_target_pairs={{0,12},{1,13},{2,14},{3,15},{4,0},{5,1},{6,2},{7,3},{8,4},{9,5},{1... | collective-permute-start | bytes 1179656 | tf_op jit(solution)/shard_map/ppermute | solution.py:257
  10.2 34.7 %collective-permute-start.17 = (bf16[512,512]{1,0:T(8,128)(2,1)}, bf16[512,512]{1,0:T(8,128)(2,1)S(1)}, u32[]{:S(2)}, u32[]{:S(2)}) collective-permute-start(bf16[512,512]{1,0:T(8,128)(2,1)} %get-tuple-element.27.refs_0_), channel_id=1, source_target_pairs={{0,48},{16,0},{32,16},{48,32},{64,112},{80,64},{96,80},{112,96},{1... | collective-permute-start | bytes 1572872 | tf_op jit(solution)/shard_map/ppermute | solution.py:250
  12.7 16.9 %collective-permute-start.2 = (bf16[3,64,1024]{2,1,0:T(8,128)(2,1)}, bf16[3,64,1024]{2,1,0:T(8,128)(2,1)S(1)}, u32[]{:S(2)}, u32[]{:S(2)}) collective-permute-start(bf16[3,64,1024]{2,1,0:T(8,128)(2,1)} %get-tuple-element.23.refs_0_), channel_id=1, source_target_pairs={{0,4},{1,5},{2,6},{3,7},{4,8},{5,9},{6,10},{7,11},{8,12},{9,13},{1... | collective-permute-start | bytes 1179656 | tf_op jit(solution)/shard_map/ppermute | solution.py:257
  12.7 24.2 %collective-permute-start.1 = (bf16[3,64,1024]{2,1,0:T(8,128)(2,1)}, bf16[3,64,1024]{2,1,0:T(8,128)(2,1)S(1)}, u32[]{:S(2)}, u32[]{:S(2)}) collective-permute-start(bf16[3,64,1024]{2,1,0:T(8,128)(2,1)} %get-tuple-element.23.refs_0_), channel_id=1, source_target_pairs={{0,14},{1,15},{2,0},{3,1},{4,2},{5,3},{6,4},{7,5},{8,6},{9,7},{10,... | collective-permute-start | bytes 1179656 | tf_op jit(solution)/shard_map/ppermute | solution.py:257
  15.8 26.2 %collective-permute-start = (bf16[3,64,1024]{2,1,0:T(8,128)(2,1)}, bf16[3,64,1024]{2,1,0:T(8,128)(2,1)S(1)}, u32[]{:S(2)}, u32[]{:S(2)}) collective-permute-start(bf16[3,64,1024]{2,1,0:T(8,128)(2,1)} %get-tuple-element.23.refs_0_), channel_id=1, source_target_pairs={{0,2},{1,3},{2,4},{3,5},{4,6},{5,7},{6,8},{7,9},{8,10},{9,11},{10,... | collective-permute-start | bytes 1179656 | tf_op jit(solution)/shard_map/ppermute | solution.py:257
  26.2 20.0 %collective-permute-start.16 = (bf16[512,512]{1,0:T(8,128)(2,1)}, bf16[512,512]{1,0:T(8,128)(2,1)S(1)}, u32[]{:S(2)}, u32[]{:S(2)}) collective-permute-start(bf16[512,512]{1,0:T(8,128)(2,1)} %get-tuple-element.27.refs_0_), channel_id=1, source_target_pairs={{0,32},{16,48},{32,0},{48,16},{64,96},{80,112},{96,64},{112,80},{1... | collective-permute-start | bytes 1572872 | tf_op jit(solution)/shard_map/ppermute | solution.py:250
  29.6 23.9 %collective-permute-start.15 = (bf16[512,512]{1,0:T(8,128)(2,1)}, bf16[512,512]{1,0:T(8,128)(2,1)S(1)}, u32[]{:S(2)}, u32[]{:S(2)}) collective-permute-start(bf16[512,512]{1,0:T(8,128)(2,1)} %get-tuple-element.27.refs_0_), channel_id=1, source_target_pairs={{0,16},{16,32},{32,48},{48,0},{64,80},{80,96},{96,112},{112,64},{1... | collective-permute-start | bytes 1572872 | tf_op jit(solution)/shard_map/ppermute | solution.py:250
  36.9 21.7 %collective-permute-start.23 = (bf16[512,512]{1,0:T(8,128)(2,1)}, bf16[512,512]{1,0:T(8,128)(2,1)S(1)}, u32[]{:S(2)}, u32[]{:S(2)}) collective-permute-start(bf16[512,512]{1,0:T(8,128)(2,1)} %get-tuple-element.32.refs_0_), channel_id=1, source_target_pairs={{0,192},{16,208},{32,224},{48,240},{64,0},{80,16},{96,32},{112,48}... | collective-permute-start | bytes 1572872 | tf_op jit(solution)/shard_map/ppermute | solution.py:250
  42.0 21.1 %collective-permute-start.22 = (bf16[512,512]{1,0:T(8,128)(2,1)}, bf16[512,512]{1,0:T(8,128)(2,1)}, u32[]{:S(2)}, u32[]{:S(2)}) collective-permute-start(bf16[512,512]{1,0:T(8,128)(2,1)} %get-tuple-element.32.refs_0_), channel_id=1, source_target_pairs={{0,128},{16,144},{32,160},{48,176},{64,192},{80,208},{96,224},{112... | collective-permute-start | bytes 1572872 | tf_op jit(solution)/shard_map/ppermute | solution.py:250
  45.7 23.2 %collective-permute-start.21 = (bf16[512,512]{1,0:T(8,128)(2,1)}, bf16[512,512]{1,0:T(8,128)(2,1)}, u32[]{:S(2)}, u32[]{:S(2)}) collective-permute-start(bf16[512,512]{1,0:T(8,128)(2,1)} %get-tuple-element.32.refs_0_), channel_id=1, source_target_pairs={{0,64},{16,80},{32,96},{48,112},{64,128},{80,144},{96,160},{112,17... | collective-permute-start | bytes 1572872 | tf_op jit(solution)/shard_map/ppermute | solution.py:250
  46.9 22.0 %collective-permute-start.11 = (bf16[3,64,1024]{2,1,0:T(8,128)(2,1)S(1)}, bf16[3,64,1024]{2,1,0:T(8,128)(2,1)S(1)}, u32[]{:S(2)}, u32[]{:S(2)}) collective-permute-start(bf16[3,64,1024]{2,1,0:T(8,128)(2,1)S(1)} %collective-permute-done.3.refs_4_), channel_id=1, source_target_pairs={{0,1},{1,0},{2,3},{3,2},{4,5},{5,4},{6,7},{7,6},{8,9},{9,8},{10,11... | collective-permute-start | bytes 1179656 | tf_op jit(solution)/shard_map/ppermute | solution.py:261
  54.3 36.1 %collective-permute-start.5 = (bf16[3,64,1024]{2,1,0:T(8,128)(2,1)S(1)}, bf16[3,64,1024]{2,1,0:T(8,128)(2,1)S(1)}, u32[]{:S(2)}, u32[]{:S(2)}) collective-permute-start(bf16[3,64,1024]{2,1,0:T(8,128)(2,1)S(1)} %collective-permute-done.3.refs_4_), channel_id=1, source_target_pairs={{0,14},{1,15},{2,0},{3,1},{4,2},{5,3},{6,4},{7,5},{8,6},{9,7},{10,... | collective-permute-start | bytes 1179656 | tf_op jit(solution)/shard_map/ppermute | solution.py:257
  59.4 31.3 %collective-permute-start.10 = (bf16[3,64,1024]{2,1,0:T(8,128)(2,1)S(1)}, bf16[3,64,1024]{2,1,0:T(8,128)(2,1)S(1)}, u32[]{:S(2)}, u32[]{:S(2)}) collective-permute-start(bf16[3,64,1024]{2,1,0:T(8,128)(2,1)S(1)} %collective-permute-done.2.refs_3_), channel_id=1, source_target_pairs={{0,1},{1,0},{2,3},{3,2},{4,5},{5,4},{6,7},{7,6},{8,9},{9,8},{10,11... | collective-permute-start | bytes 1179656 | tf_op jit(solution)/shard_map/ppermute | solution.py:261
  63.1 29.3 %collective-permute-start.6 = (bf16[3,64,1024]{2,1,0:T(8,128)(2,1)S(1)}, bf16[3,64,1024]{2,1,0:T(8,128)(2,1)S(1)}, u32[]{:S(2)}, u32[]{:S(2)}) collective-permute-start(bf16[3,64,1024]{2,1,0:T(8,128)(2,1)S(1)} %collective-permute-done.2.refs_3_), channel_id=1, source_target_pairs={{0,4},{1,5},{2,6},{3,7},{4,8},{5,9},{6,10},{7,11},{8,12},{9,13},{1... | collective-permute-start | bytes 1179656 | tf_op jit(solution)/shard_map/ppermute | solution.py:257
  68.9 23.8 %collective-permute-start.4 = (bf16[3,64,1024]{2,1,0:T(8,128)(2,1)S(1)}, bf16[3,64,1024]{2,1,0:T(8,128)(2,1)}, u32[]{:S(2)}, u32[]{:S(2)}) collective-permute-start(bf16[3,64,1024]{2,1,0:T(8,128)(2,1)S(1)} %collective-permute-done.2.refs_3_), channel_id=1, source_target_pairs={{0,2},{1,3},{2,4},{3,5},{4,6},{5,7},{6,8},{7,9},{8,10},{9,11},{10,... | collective-permute-start | bytes 1179656 | tf_op jit(solution)/shard_map/ppermute | solution.py:257
  68.9 24.4 %collective-permute-start.9 = (bf16[3,64,1024]{2,1,0:T(8,128)(2,1)S(1)}, bf16[3,64,1024]{2,1,0:T(8,128)(2,1)}, u32[]{:S(2)}, u32[]{:S(2)}) collective-permute-start(bf16[3,64,1024]{2,1,0:T(8,128)(2,1)S(1)} %collective-permute-done.1.refs_2_), channel_id=1, source_target_pairs={{0,1},{1,0},{2,3},{3,2},{4,5},{5,4},{6,7},{7,6},{8,9},{9,8},{10,11... | collective-permute-start | bytes 1179656 | tf_op jit(solution)/shard_map/ppermute | solution.py:261
  90.4 14.0 %collective-permute-start.18 = (bf16[512,512]{1,0:T(8,128)(2,1)S(1)}, bf16[512,512]{1,0:T(8,128)(2,1)S(1)}, u32[]{:S(2)}, u32[]{:S(2)}) collective-permute-start(bf16[512,512]{1,0:T(8,128)(2,1)S(1)} %get-tuple-element.29), channel_id=1, source_target_pairs={{0,64},{16,80},{32,96},{48,112},{64,128},{80,144},{96,160},{112,17... | collective-permute-start | bytes 1572872 | tf_op jit(solution)/shard_map/ppermute | solution.py:250
  93.3 13.2 %collective-permute-start.12 = (bf16[3,64,1024]{2,1,0:T(8,128)(2,1)}, bf16[3,64,1024]{2,1,0:T(8,128)(2,1)S(1)}, u32[]{:S(2)}, u32[]{:S(2)}) collective-permute-start(bf16[3,64,1024]{2,1,0:T(8,128)(2,1)} %collective-permute-done.4.refs_5_), channel_id=1, source_target_pairs={{0,1},{1,0},{2,3},{3,2},{4,5},{5,4},{6,7},{7,6},{8,9},{9,8},{10,11... | collective-permute-start | bytes 1179656 | tf_op jit(solution)/shard_map/ppermute | solution.py:261
  96.1 18.2 %collective-permute-start.19 = (bf16[512,512]{1,0:T(8,128)(2,1)S(1)}, bf16[512,512]{1,0:T(8,128)(2,1)S(1)}, u32[]{:S(2)}, u32[]{:S(2)}) collective-permute-start(bf16[512,512]{1,0:T(8,128)(2,1)S(1)} %get-tuple-element.30), channel_id=1, source_target_pairs={{0,128},{16,144},{32,160},{48,176},{64,192},{80,208},{96,224},{112... | collective-permute-start | bytes 1572872 | tf_op jit(solution)/shard_map/ppermute | solution.py:250
  104.4 13.6 %collective-permute-start.20 = (bf16[512,512]{1,0:T(8,128)(2,1)S(1)}, bf16[512,512]{1,0:T(8,128)(2,1)S(1)}, u32[]{:S(2)}, u32[]{:S(2)}) collective-permute-start(bf16[512,512]{1,0:T(8,128)(2,1)S(1)} %get-tuple-element.31), channel_id=1, source_target_pairs={{0,192},{16,208},{32,224},{48,240},{64,0},{80,16},{96,32},{112,48}... | collective-permute-start | bytes 1572872 | tf_op jit(solution)/shard_map/ppermute | solution.py:250
  104.4 14.9 %collective-permute-start.24 = (bf16[512,512]{1,0:T(8,128)(2,1)S(1)}, bf16[512,512]{1,0:T(8,128)(2,1)S(1)}, u32[]{:S(2)}, u32[]{:S(2)}) collective-permute-start(bf16[512,512]{1,0:T(8,128)(2,1)S(1)} %get-tuple-element.34), channel_id=1, source_target_pairs={{0,16},{16,32},{32,48},{48,0},{64,80},{80,96},{96,112},{112,64},{1... | collective-permute-start | bytes 1572872 | tf_op jit(solution)/shard_map/ppermute | solution.py:250
  104.6 14.6 %collective-permute-start.25 = (bf16[512,512]{1,0:T(8,128)(2,1)S(1)}, bf16[512,512]{1,0:T(8,128)(2,1)S(1)}, u32[]{:S(2)}, u32[]{:S(2)}) collective-permute-start(bf16[512,512]{1,0:T(8,128)(2,1)S(1)} %get-tuple-element.35), channel_id=1, source_target_pairs={{0,32},{16,48},{32,0},{48,16},{64,96},{80,112},{96,64},{112,80},{1... | collective-permute-start | bytes 1572872 | tf_op jit(solution)/shard_map/ppermute | solution.py:250
  106.5 13.3 %collective-permute-start.26 = (bf16[512,512]{1,0:T(8,128)(2,1)S(1)}, bf16[512,512]{1,0:T(8,128)(2,1)S(1)}, u32[]{:S(2)}, u32[]{:S(2)}) collective-permute-start(bf16[512,512]{1,0:T(8,128)(2,1)S(1)} %get-tuple-element.36), channel_id=1, source_target_pairs={{0,48},{16,0},{32,16},{48,32},{64,112},{80,64},{96,80},{112,96},{1... | collective-permute-start | bytes 1572872 | tf_op jit(solution)/shard_map/ppermute | solution.py:250
  (16 other events, 89.7 us)
where the time goes:
time: 205 us; the launch traced here: 202 us
  blocking collectives  61.6 us (30%)
  waiting for transfers between devices  55.3 us (27%)
  starting transfers between devices  44.5 us (22%)
  Pallas kernels  32.3 us (16%)
  local copies, waits for them, and re-layouts  7.39 us (4%)
    all_to_all x1, blocking collectives, layer(): lax.all_to_all(produced, 'ep', split_axis=0, concat_axis=0, tiled=True)  61.6 us
    ppermute x12, waiting for transfers between devices, over_plane(): lax.ppermute(array, 'ep', [(y * SIDE + x, (y + by_y) % SIDE * SIDE + (x +...  27.8 us
    ppermute x7, waiting for transfers between devices, along_z(): lax.ppermute(array, 'tp', [(z * 2 + c, (z + by) % chips * 2 + c) for z in...  21 us
    ppermute x12, starting transfers between devices, over_plane(): lax.ppermute(array, 'ep', [(y * SIDE + x, (y + by_y) % SIDE * SIDE + (x +...  16.8 us
    pallas_call x1, Pallas kernels, expert(): pl.pallas_call(expert_kernel, grid_spec=pltpu.PrefetchScalarGridSpec(num_...  14.8 us
    ppermute x7, starting transfers between devices, along_z(): lax.ppermute(array, 'tp', [(z * 2 + c, (z + by) % chips * 2 + c) for z in...  11.7 us
    ppermute x8, starting transfers between devices, other_core(): return lax.ppermute(array, 'tp', [(j, j ^ 1) for j in range(tp_count)])  11.4 us
    unnamed x24, local copies, waits for them, and re-layouts  7.39 us
  transfers between devices with their start and end apart: 28, of which 12 were waited for; matrix products, arithmetic and copies ran while one was open for 0% of the time, Pallas kernels for 5%

commit v1 on v0

--- a/solution.py
+++ b/solution.py
@@ -138,14 +138,16 @@
 
 def assemble_kernel(*refs):
     pieces, outs = refs[:-3], refs[-3:]
-    width = pieces[0].shape[1]
-    for k, piece in enumerate(pieces):
+    at = 0
+    for piece in pieces:
+        width = piece.shape[1]
         for j, out in enumerate(outs):
-            out[k * width : (k + 1) * width, :] = piece[j]
+            out[at : at + width, :] = piece[j]
+        at += width
 
 
 def assemble(pieces):
-    shape = jax.ShapeDtypeStruct((len(pieces) * pieces[0].shape[1], pieces[0].shape[2]), jnp.bfloat16)
+    shape = jax.ShapeDtypeStruct((sum(piece.shape[1] for piece in pieces), pieces[0].shape[2]), jnp.bfloat16)
     return pl.pallas_call(
         assemble_kernel,
         in_specs=[VMEM] * len(pieces),
@@ -272,15 +274,22 @@
     low, high, own = prepare(stream, norm_gain, (gate_rows, up_rows, down_rows))
     lows = [low] + [over_plane(low, 0, t) for t in range(1, SIDE)]
     highs = [high] + [over_plane(high, t, 0) for t in range(1, SIDE)]
+    ahead, behind = along_z(own, 1, tp_count), along_z(own, -1, tp_count)
     rows_there, weights = windows(bounds, chosen, affinity, block, slots)
     rows_here = lax.all_to_all(rows_there, "ep", split_axis=0, concat_axis=0, tiled=True)
-    near = {by: along_z(own, by, tp_count) for by in (1, -1, 2, -2)}
+    ahead2, behind2 = along_z(ahead, 1, tp_count), along_z(behind, -1, tp_count)
     picked_low = pick(True, place, rows_here, lows)
     arrived_low = [picked_low[0]] + [over_plane(picked_low[d], d, 0) for d in range(1, SIDE)]
     picked_high = pick(False, place, rows_here, highs)
     arrived_high = [picked_high[0]] + [over_plane(picked_high[d], 0, d) for d in range(1, SIDE)]
-    far = [along_z(near[2], 1, tp_count), along_z(near[-2], -1, tp_count), along_z(near[2], 2, tp_count)]
-    held = [own, *near.values(), *far]
+    cut = own.shape[1] // 2
+    far = [
+        along_z(ahead2[:, :cut], 2, tp_count),
+        along_z(behind2[:, cut:], -2, tp_count),
+        along_z(ahead2, 1, tp_count),
+        along_z(behind2, -1, tp_count),
+    ]
+    held = [own, ahead, behind, ahead2, behind2, *far]
     pieces = held + [other_core(piece, tp_count) for piece in held]
     produced = expert(place, weights, arrived_low, arrived_high, *assemble(pieces))
     returned = lax.all_to_all(produced, "ep", split_axis=0, concat_axis=0, tiled=True)

time: 205 us -> 195 us (0.951)
  waiting for transfers between devices: 55.3 us -> 44.2 us
  starting transfers between devices: 44.5 us -> 54.7 us
  blocking collectives: 61.6 us -> 56.3 us
  Pallas kernels: 32.3 us -> 30 us
    all_to_all x1, blocking collectives: 61.6 us -> 56.3 us  [layer(): lax.all_to_all(produced, 'ep', split_axis=0, concat_axis=0, tiled=True)]
    ppermute x7 -> x8, starting transfers between devices: 11.7 us -> 16.3 us  [along_z(): lax.ppermute(array, 'tp', [(z * 2 + c, (z + by) % chips * 2 + c) for z in...]
    ppermute x7 -> x8, waiting for transfers between devices: 21 us -> 16.5 us  [along_z(): lax.ppermute(array, 'tp', [(z * 2 + c, (z + by) % chips * 2 + c) for z in...]
    ppermute x12, waiting for transfers between devices: 27.8 us -> 23.4 us  [over_plane(): lax.ppermute(array, 'ep', [(y * SIDE + x, (y + by_y) % SIDE * SIDE + (x +...]
    ppermute x8 -> x9, starting transfers between devices: 11.4 us -> 14.6 us  [other_core(): return lax.ppermute(array, 'tp', [(j, j ^ 1) for j in range(tp_count)])]
    all_to_all x1, waiting for transfers between devices: 6.47 us -> 3.82 us  [layer(): lax.all_to_all(rows_there, 'ep', split_axis=0, concat_axis=0, tiled=True)]
  transfers between devices with their start and end apart: 28 -> 30, of which waited for: 12 -> 10; matrix products, arithmetic and copies ran while one was open for 0% -> 0% of each run, Pallas kernels for 5% -> 4%
where the time goes in v1:
time: 195 us; the launch traced here: 193 us
  blocking collectives  56.3 us (29%)
  starting transfers between devices  54.7 us (28%)
  waiting for transfers between devices  44.2 us (23%)
  Pallas kernels  30 us (15%)
  local copies, waits for them, and re-layouts  7.43 us (4%)
    all_to_all x1, blocking collectives, layer(): lax.all_to_all(produced, 'ep', split_axis=0, concat_axis=0, tiled=True)  56.3 us
    ppermute x12, waiting for transfers between devices, over_plane(): lax.ppermute(array, 'ep', [(y * SIDE + x, (y + by_y) % SIDE * SIDE + (x +...  23.4 us
    ppermute x12, starting transfers between devices, over_plane(): lax.ppermute(array, 'ep', [(y * SIDE + x, (y + by_y) % SIDE * SIDE + (x +...  18 us
    ppermute x8, waiting for transfers between devices, along_z(): lax.ppermute(array, 'tp', [(z * 2 + c, (z + by) % chips * 2 + c) for z in...  16.5 us
    ppermute x8, starting transfers between devices, along_z(): lax.ppermute(array, 'tp', [(z * 2 + c, (z + by) % chips * 2 + c) for z in...  16.3 us
    pallas_call x1, Pallas kernels, expert(): pl.pallas_call(expert_kernel, grid_spec=pltpu.PrefetchScalarGridSpec(num_...  14.8 us
    ppermute x9, starting transfers between devices, other_core(): return lax.ppermute(array, 'tp', [(j, j ^ 1) for j in range(tp_count)])  14.6 us
    unnamed x24, local copies, waits for them, and re-layouts  7.4 us
  transfers between devices with their start and end apart: 30, of which 10 were waited for; matrix products, arithmetic and copies ran while one was open for 0% of the time, Pallas kernels for 4%

profile of v1, /device:TPU:1, one launch (start us, length us, event | category | flops | bytes accessed | tf_op | source)
XLA Modules:
  0.0 193.4 jit_solution(17345972474312153002)
XLA Ops:
  0.0 2.6 %prepare.1 = (bf16[512,512]{1,0:T(8,128)(2,1)}, bf16[512,512]{1,0:T(8,128)(2,1)}, bf16[3,64,1024]{2,1,0:T(8,128)(2,1)}) custom-call(bf16[512,1024]{1,0:T(8,128)(2,1)} %stream_ref.1, f32[1,1024]{1,0:T(1,128)} %bitcast.9, bf16[1,64,1024]{2,1,0:T(8,128)(2,1)} %gate_ref.1, bf16[1,64,1024]{2,1,0:T(8,128)(2,1)} %up_ref.1, bf16[1,64,1024]{2,1,0:T(8,128)(2,1)} %down_ref.1), custom_call_target="tpu_custom_call" | custom-call | flops 3000000 | bytes 3145728 | tf_op jit(solution)/shard_map/prepare/pallas_call | solution.py:80
  2.6 3.3 %collective-permute-start.8 = (bf16[3,64,1024]{2,1,0:T(8,128)(2,1)}, bf16[3,64,1024]{2,1,0:T(8,128)(2,1)S(1)}, u32[]{:S(2)}, u32[]{:S(2)}) collective-permute-start(bf16[3,64,1024]{2,1,0:T(8,128)(2,1)} %get-tuple-element.23.refs_0_), channel_id=1, source_target_pairs={{0,1},{1,0},{2,3},{3,2},{4,5},{5,4},{6,7},{7,6},{8,9},{9,8},{10,11... | collective-permute-start | bytes 1179656 | tf_op jit(solution)/shard_map/ppermute | solution.py:263
  6.6 5.6 %collective-permute-start.1 = (bf16[3,64,1024]{2,1,0:T(8,128)(2,1)}, bf16[3,64,1024]{2,1,0:T(8,128)(2,1)S(1)}, u32[]{:S(2)}, u32[]{:S(2)}) collective-permute-start(bf16[3,64,1024]{2,1,0:T(8,128)(2,1)} %get-tuple-element.23.refs_0_), channel_id=1, source_target_pairs={{0,14},{1,15},{2,0},{3,1},{4,2},{5,3},{6,4},{7,5},{8,6},{9,7},{10,... | collective-permute-start | bytes 1179656 | tf_op jit(solution)/shard_map/ppermute | solution.py:259
  13.4 7.3 %collective-permute-done.1.refs_2_ = bf16[3,64,1024]{2,1,0:T(8,128)(2,1)S(1)} collective-permute-done((bf16[3,64,1024]{2,1,0:T(8,128)(2,1)}, bf16[3,64,1024]{2,1,0:T(8,128)(2,1)S(1)}, u32[]{:S(2)}, u32[]{:S(2)}) %collective-permute-start.1) | collective-permute-done | bytes 393248 | tf_op jit(solution)/shard_map/ppermute | solution.py:259
  20.6 2.7 %collective-permute-start.25 = (bf16[512,512]{1,0:T(8,128)(2,1)}, bf16[512,512]{1,0:T(8,128)(2,1)S(1)}, u32[]{:S(2)}, u32[]{:S(2)}) collective-permute-start(bf16[512,512]{1,0:T(8,128)(2,1)} %get-tuple-element.32.refs_0_), channel_id=1, source_target_pairs={{0,192},{16,208},{32,224},{48,240},{64,0},{80,16},{96,32},{112,48}... | collective-permute-start | bytes 1572872 | tf_op jit(solution)/shard_map/ppermute | solution.py:252
  23.7 2.9 %collective-permute-start.24 = (bf16[512,512]{1,0:T(8,128)(2,1)}, bf16[512,512]{1,0:T(8,128)(2,1)}, u32[]{:S(2)}, u32[]{:S(2)}) collective-permute-start(bf16[512,512]{1,0:T(8,128)(2,1)} %get-tuple-element.32.refs_0_), channel_id=1, source_target_pairs={{0,128},{16,144},{32,160},{48,176},{64,192},{80,208},{96,224},{112... | collective-permute-start | bytes 1572872 | tf_op jit(solution)/shard_map/ppermute | solution.py:252
  27.4 4.0 %collective-permute-start.23 = (bf16[512,512]{1,0:T(8,128)(2,1)}, bf16[512,512]{1,0:T(8,128)(2,1)}, u32[]{:S(2)}, u32[]{:S(2)}) collective-permute-start(bf16[512,512]{1,0:T(8,128)(2,1)} %get-tuple-element.32.refs_0_), channel_id=1, source_target_pairs={{0,64},{16,80},{32,96},{48,112},{64,128},{80,144},{96,160},{112,17... | collective-permute-start | bytes 1572872 | tf_op jit(solution)/shard_map/ppermute | solution.py:252
  32.2 5.6 %collective-permute-start.3 = (bf16[3,64,1024]{2,1,0:T(8,128)(2,1)S(1)}, bf16[3,64,1024]{2,1,0:T(8,128)(2,1)S(1)}, u32[]{:S(2)}, u32[]{:S(2)}) collective-permute-start(bf16[3,64,1024]{2,1,0:T(8,128)(2,1)S(1)} %collective-permute-done.1.refs_2_), channel_id=1, source_target_pairs={{0,14},{1,15},{2,0},{3,1},{4,2},{5,3},{6,4},{7,5},{8,6},{9,7},{10,... | collective-permute-start | bytes 1179656 | tf_op jit(solution)/shard_map/ppermute | solution.py:259
  40.5 2.6 %windows.1 = (s32[16,8,128]{2,1,0:T(8,128)}, f32[16,128]{1,0:T(8,128)}) custom-call(s32[16]{0:T(128)} %add_multiply_fusion.bounds_ref, s32[128,128]{1,0:T(8,128)} %bitcast.7, f32[128,128]{1,0:T(8,128)} %bitcast.8), custom_call_target="tpu_custom_call" | custom-call | flops 8000000 | bytes 150000 | tf_op jit(solution)/shard_map/windows/pallas_call | solution.py:48
  43.0 5.8 %all-to-all-start = ((s32[16,8,128]{2,1,0:T(8,128)}), s32[16,8,128]{2,1,0:T(8,128)S(1)}, u32[]{:S(2)}, u32[]{:S(2)}) async-start(s32[16,8,128]{2,1,0:T(8,128)} %get-tuple-element.21), calls=%async_computation | async-start | bytes 131072 | tf_op jit(solution)/shard_map/all_to_all | solution.py:279
  49.7 1.8 collective-permute-start.10
  51.5 3.8 %all-to-all-done.rows_ref = s32[16,8,128]{2,1,0:T(8,128)S(1)} async-done(((s32[16,8,128]{2,1,0:T(8,128)}), s32[16,8,128]{2,1,0:T(8,128)S(1)}, u32[]{:S(2)}, u32[]{:S(2)}) %all-to-all-start) | async-done | bytes 65568 | tf_op jit(solution)/shard_map/all_to_all | solution.py:279
  59.5 2.1 %pick_y.1 = (bf16[512,512]{1,0:T(8,128)(2,1)S(1)}, bf16[512,512]{1,0:T(8,128)(2,1)S(1)}, bf16[512,512]{1,0:T(8,128)(2,1)S(1)}, bf16[512,512]{1,0:T(8,128)(2,1)S(1)}) custom-call(s32[2]{0:T(128)S(1)} %pad_add_fusion.place_ref, s32[16,8,128]{2,1,0:T(8,128)S(1)} %all-to-all-done.rows_ref, bf16[512,512]{1,0:T(8,128)(2,1)S(1)} %copy-done.4, ...), custom_call_target="tpu_custom_call" | custom-call | flops 1073741824 | bytes 4194304 | tf_op jit(solution)/shard_map/pick_y/pallas_call | solution.py:127
  61.9 2.7 %collective-permute-start.7 = (bf16[3,64,1024]{2,1,0:T(8,128)(2,1)S(1)}, bf16[3,64,1024]{2,1,0:T(8,128)(2,1)S(1)}, u32[]{:S(2)}, u32[]{:S(2)}) collective-permute-start(bf16[3,64,1024]{2,1,0:T(8,128)(2,1)S(1)} %collective-permute-done.3.refs_4_), channel_id=1, source_target_pairs={{0,14},{1,15},{2,0},{3,1},{4,2},{5,3},{6,4},{7,5},{8,6},{9,7},{10,... | collective-permute-start | bytes 1179656 | tf_op jit(solution)/shard_map/ppermute | solution.py:259
  67.2 8.9 %collective-permute-done.5.refs_6_ = bf16[3,32,1024]{2,1,0:T(8,128)(2,1)S(1)} collective-permute-done((bf16[3,32,1024]{2,1,0:T(8,128)(2,1)S(1)}, bf16[3,32,1024]{2,1,0:T(8,128)(2,1)S(1)}, u32[]{:S(2)}, u32[]{:S(2)}) %collective-permute-start.5) | collective-permute-done | bytes 196640 | tf_op jit(solution)/shard_map/ppermute | solution.py:259
  76.1 6.3 %collective-permute-start.12 = (bf16[3,64,1024]{2,1,0:T(8,128)(2,1)S(1)}, bf16[3,64,1024]{2,1,0:T(8,128)(2,1)S(1)}, u32[]{:S(2)}, u32[]{:S(2)}) collective-permute-start(bf16[3,64,1024]{2,1,0:T(8,128)(2,1)S(1)} %collective-permute-done.3.refs_4_), channel_id=1, source_target_pairs={{0,1},{1,0},{2,3},{3,2},{4,5},{5,4},{6,7},{7,6},{8,9},{9,8},{10,11... | collective-permute-start | bytes 1179656 | tf_op jit(solution)/shard_map/ppermute | solution.py:263
  82.4 2.2 %collective-permute-start.14 = (bf16[3,32,1024]{2,1,0:T(8,128)(2,1)S(1)}, bf16[3,32,1024]{2,1,0:T(8,128)(2,1)S(1)}, u32[]{:S(2)}, u32[]{:S(2)}) collective-permute-start(bf16[3,32,1024]{2,1,0:T(8,128)(2,1)S(1)} %collective-permute-done.5.refs_6_), channel_id=1, source_target_pairs={{0,1},{1,0},{2,3},{3,2},{4,5},{5,4},{6,7},{7,6},{8,9},{9,8},{10,11... | collective-permute-start | bytes 589832 | tf_op jit(solution)/shard_map/ppermute | solution.py:263
  86.1 2.7 %pick_x.1 = (bf16[512,512]{1,0:T(8,128)(2,1)S(1)}, bf16[512,512]{1,0:T(8,128)(2,1)S(1)}, bf16[512,512]{1,0:T(8,128)(2,1)S(1)}, bf16[512,512]{1,0:T(8,128)(2,1)S(1)}) custom-call(s32[2]{0:T(128)S(1)} %pad_add_fusion.place_ref, s32[16,8,128]{2,1,0:T(8,128)S(1)} %all-to-all-done.rows_ref, bf16[512,512]{1,0:T(8,128)(2,1)S(1)} %copy-done.1, ...), custom_call_target="tpu_custom_call" | custom-call | flops 1073741824 | bytes 4194304 | tf_op jit(solution)/shard_map/pick_x/pallas_call | solution.py:127
  88.9 1.8 collective-permute-start.21
  95.5 8.3 %collective-permute-done.21.refs_2_ = bf16[512,512]{1,0:T(8,128)(2,1)S(1)} collective-permute-done((bf16[512,512]{1,0:T(8,128)(2,1)S(1)}, bf16[512,512]{1,0:T(8,128)(2,1)S(1)}, u32[]{:S(2)}, u32[]{:S(2)}) %collective-permute-start.21) | collective-permute-done | bytes 524320 | tf_op jit(solution)/shard_map/ppermute | solution.py:252
  103.8 11.3 %collective-permute-done.22.refs_3_ = bf16[512,512]{1,0:T(8,128)(2,1)S(1)} collective-permute-done((bf16[512,512]{1,0:T(8,128)(2,1)S(1)}, bf16[512,512]{1,0:T(8,128)(2,1)S(1)}, u32[]{:S(2)}, u32[]{:S(2)}) %collective-permute-start.22) | collective-permute-done | bytes 524320 | tf_op jit(solution)/shard_map/ppermute | solution.py:252
  117.5 14.8 %expert.1 = bf16[16,128,1024]{2,1,0:T(8,128)(2,1)S(1)} custom-call(s32[2]{0:T(128)S(1)} %pad_add_fusion.place_ref, f32[16,128]{1,0:T(8,128)S(1)} %copy-done.11, bf16[1024,1024]{1,0:T(8,128)(2,1)S(1)} %get-tuple-element.24.gate_ref, bf16[1024,1024]{1,0:T(8,128)(2,1)S(1)} %get-tuple-element.25.up_ref, bf16[1024,1024]{1,0:T(8,128)(2,1)S(1)} %get-tuple-element.26.down_ref, ...), custom_call_target="tpu_custom_call" | custom-call | flops 12884901888 | bytes 14680064 | tf_op jit(solution)/shard_map/expert/pallas_call | solution.py:196
  132.3 56.3 %all_to_all.10 = bf16[16,128,1024]{2,1,0:T(8,128)(2,1)S(1)} all-to-all(bf16[16,128,1024]{2,1,0:T(8,128)(2,1)S(1)} %expert.1), channel_id=1, replica_groups=mesh['ep'=16,'tp'=16] {'ep'}, dimensions={0} | all-to-all | bytes 8388608 | tf_op jit(solution)/shard_map/all_to_all | solution.py:295
  188.7 4.8 %combine.1 = bf16[512,1024]{1,0:T(8,128)(2,1)} custom-call(s32[16,8,128]{2,1,0:T(8,128)S(1)} %all-to-all-done.rows_ref, bf16[2048,1024]{1,0:T(8,128)(2,1)S(1)} %bitcast.6), custom_call_target="tpu_custom_call" | custom-call | flops 2147483648 | bytes 4194304 | tf_op jit(solution)/shard_map/combine/pallas_call | solution.py:232
  (72 shorter events, 23.1 us)
Async XLA Ops:
  5.9 20.7 %collective-permute-start.19 = (bf16[512,512]{1,0:T(8,128)(2,1)}, bf16[512,512]{1,0:T(8,128)(2,1)S(1)}, u32[]{:S(2)}, u32[]{:S(2)}) collective-permute-start(bf16[512,512]{1,0:T(8,128)(2,1)} %get-tuple-element.27.refs_0_), channel_id=1, source_target_pairs={{0,48},{16,0},{32,16},{48,32},{64,112},{80,64},{96,80},{112,96},{1... | collective-permute-start | bytes 1572872 | tf_op jit(solution)/shard_map/ppermute | solution.py:252
  6.6 14.0 %collective-permute-start.1 = (bf16[3,64,1024]{2,1,0:T(8,128)(2,1)}, bf16[3,64,1024]{2,1,0:T(8,128)(2,1)S(1)}, u32[]{:S(2)}, u32[]{:S(2)}) collective-permute-start(bf16[3,64,1024]{2,1,0:T(8,128)(2,1)} %get-tuple-element.23.refs_0_), channel_id=1, source_target_pairs={{0,14},{1,15},{2,0},{3,1},{4,2},{5,3},{6,4},{7,5},{8,6},{9,7},{10,... | collective-permute-start | bytes 1179656 | tf_op jit(solution)/shard_map/ppermute | solution.py:259
  12.2 11.4 %collective-permute-start = (bf16[3,64,1024]{2,1,0:T(8,128)(2,1)}, bf16[3,64,1024]{2,1,0:T(8,128)(2,1)S(1)}, u32[]{:S(2)}, u32[]{:S(2)}) collective-permute-start(bf16[3,64,1024]{2,1,0:T(8,128)(2,1)} %get-tuple-element.23.refs_0_), channel_id=1, source_target_pairs={{0,2},{1,3},{2,4},{3,5},{4,6},{5,7},{6,8},{7,9},{8,10},{9,11},{10,... | collective-permute-start | bytes 1179656 | tf_op jit(solution)/shard_map/ppermute | solution.py:259
  12.2 19.1 %collective-permute-start.18 = (bf16[512,512]{1,0:T(8,128)(2,1)}, bf16[512,512]{1,0:T(8,128)(2,1)S(1)}, u32[]{:S(2)}, u32[]{:S(2)}) collective-permute-start(bf16[512,512]{1,0:T(8,128)(2,1)} %get-tuple-element.27.refs_0_), channel_id=1, source_target_pairs={{0,32},{16,48},{32,0},{48,16},{64,96},{80,112},{96,64},{112,80},{1... | collective-permute-start | bytes 1572872 | tf_op jit(solution)/shard_map/ppermute | solution.py:252
  12.8 26.4 %collective-permute-start.17 = (bf16[512,512]{1,0:T(8,128)(2,1)}, bf16[512,512]{1,0:T(8,128)(2,1)S(1)}, u32[]{:S(2)}, u32[]{:S(2)}) collective-permute-start(bf16[512,512]{1,0:T(8,128)(2,1)} %get-tuple-element.27.refs_0_), channel_id=1, source_target_pairs={{0,16},{16,32},{32,48},{48,0},{64,80},{80,96},{96,112},{112,64},{1... | collective-permute-start | bytes 1572872 | tf_op jit(solution)/shard_map/ppermute | solution.py:252
  20.6 28.3 %collective-permute-start.25 = (bf16[512,512]{1,0:T(8,128)(2,1)}, bf16[512,512]{1,0:T(8,128)(2,1)S(1)}, u32[]{:S(2)}, u32[]{:S(2)}) collective-permute-start(bf16[512,512]{1,0:T(8,128)(2,1)} %get-tuple-element.32.refs_0_), channel_id=1, source_target_pairs={{0,192},{16,208},{32,224},{48,240},{64,0},{80,16},{96,32},{112,48}... | collective-permute-start | bytes 1572872 | tf_op jit(solution)/shard_map/ppermute | solution.py:252
  23.7 27.8 %collective-permute-start.24 = (bf16[512,512]{1,0:T(8,128)(2,1)}, bf16[512,512]{1,0:T(8,128)(2,1)}, u32[]{:S(2)}, u32[]{:S(2)}) collective-permute-start(bf16[512,512]{1,0:T(8,128)(2,1)} %get-tuple-element.32.refs_0_), channel_id=1, source_target_pairs={{0,128},{16,144},{32,160},{48,176},{64,192},{80,208},{96,224},{112... | collective-permute-start | bytes 1572872 | tf_op jit(solution)/shard_map/ppermute | solution.py:252
  27.4 34.2 %collective-permute-start.23 = (bf16[512,512]{1,0:T(8,128)(2,1)}, bf16[512,512]{1,0:T(8,128)(2,1)}, u32[]{:S(2)}, u32[]{:S(2)}) collective-permute-start(bf16[512,512]{1,0:T(8,128)(2,1)} %get-tuple-element.32.refs_0_), channel_id=1, source_target_pairs={{0,64},{16,80},{32,96},{48,112},{64,128},{80,144},{96,160},{112,17... | collective-permute-start | bytes 1572872 | tf_op jit(solution)/shard_map/ppermute | solution.py:252
  32.2 29.8 %collective-permute-start.3 = (bf16[3,64,1024]{2,1,0:T(8,128)(2,1)S(1)}, bf16[3,64,1024]{2,1,0:T(8,128)(2,1)S(1)}, u32[]{:S(2)}, u32[]{:S(2)}) collective-permute-start(bf16[3,64,1024]{2,1,0:T(8,128)(2,1)S(1)} %collective-permute-done.1.refs_2_), channel_id=1, source_target_pairs={{0,14},{1,15},{2,0},{3,1},{4,2},{5,3},{6,4},{7,5},{8,6},{9,7},{10,... | collective-permute-start | bytes 1179656 | tf_op jit(solution)/shard_map/ppermute | solution.py:259
  39.9 24.7 %collective-permute-start.2 = (bf16[3,64,1024]{2,1,0:T(8,128)(2,1)S(1)}, bf16[3,64,1024]{2,1,0:T(8,128)(2,1)S(1)}, u32[]{:S(2)}, u32[]{:S(2)}) collective-permute-start(bf16[3,64,1024]{2,1,0:T(8,128)(2,1)S(1)} %collective-permute-done.refs_1_), channel_id=1, source_target_pairs={{0,2},{1,3},{2,4},{3,5},{4,6},{5,7},{6,8},{7,9},{8,10},{9,11},{10,... | collective-permute-start | bytes 1179656 | tf_op jit(solution)/shard_map/ppermute | solution.py:259
  43.0 12.3 %all-to-all-start = ((s32[16,8,128]{2,1,0:T(8,128)}), s32[16,8,128]{2,1,0:T(8,128)S(1)}, u32[]{:S(2)}, u32[]{:S(2)}) async-start(s32[16,8,128]{2,1,0:T(8,128)} %get-tuple-element.21), calls=%async_computation | async-start | bytes 131072 | tf_op jit(solution)/shard_map/all_to_all | solution.py:279
  49.7 15.0 %collective-permute-start.10 = (bf16[3,64,1024]{2,1,0:T(8,128)(2,1)S(1)}, bf16[3,64,1024]{2,1,0:T(8,128)(2,1)S(1)}, u32[]{:S(2)}, u32[]{:S(2)}) collective-permute-start(bf16[3,64,1024]{2,1,0:T(8,128)(2,1)S(1)} %collective-permute-done.1.refs_2_), channel_id=1, source_target_pairs={{0,1},{1,0},{2,3},{3,2},{4,5},{5,4},{6,7},{7,6},{8,9},{9,8},{10,11... | collective-permute-start | bytes 1179656 | tf_op jit(solution)/shard_map/ppermute | solution.py:263
  51.5 14.7 %collective-permute-start.9 = (bf16[3,64,1024]{2,1,0:T(8,128)(2,1)S(1)}, bf16[3,64,1024]{2,1,0:T(8,128)(2,1)S(1)}, u32[]{:S(2)}, u32[]{:S(2)}) collective-permute-start(bf16[3,64,1024]{2,1,0:T(8,128)(2,1)S(1)} %collective-permute-done.refs_1_), channel_id=1, source_target_pairs={{0,1},{1,0},{2,3},{3,2},{4,5},{5,4},{6,7},{7,6},{8,9},{9,8},{10,11... | collective-permute-start | bytes 1179656 | tf_op jit(solution)/shard_map/ppermute | solution.py:263
  61.6 23.0 %collective-permute-start.20 = (bf16[512,512]{1,0:T(8,128)(2,1)S(1)}, bf16[512,512]{1,0:T(8,128)(2,1)S(1)}, u32[]{:S(2)}, u32[]{:S(2)}) collective-permute-start(bf16[512,512]{1,0:T(8,128)(2,1)S(1)} %get-tuple-element.29), channel_id=1, source_target_pairs={{0,64},{16,80},{32,96},{48,112},{64,128},{80,144},{96,160},{112,17... | collective-permute-start | bytes 1572872 | tf_op jit(solution)/shard_map/ppermute | solution.py:252
  61.9 22.7 %collective-permute-start.7 = (bf16[3,64,1024]{2,1,0:T(8,128)(2,1)S(1)}, bf16[3,64,1024]{2,1,0:T(8,128)(2,1)S(1)}, u32[]{:S(2)}, u32[]{:S(2)}) collective-permute-start(bf16[3,64,1024]{2,1,0:T(8,128)(2,1)S(1)} %collective-permute-done.3.refs_4_), channel_id=1, source_target_pairs={{0,14},{1,15},{2,0},{3,1},{4,2},{5,3},{6,4},{7,5},{8,6},{9,7},{10,... | collective-permute-start | bytes 1179656 | tf_op jit(solution)/shard_map/ppermute | solution.py:259
  64.6 20.5 %collective-permute-start.6 = (bf16[3,64,1024]{2,1,0:T(8,128)(2,1)S(1)}, bf16[3,64,1024]{2,1,0:T(8,128)(2,1)S(1)}, u32[]{:S(2)}, u32[]{:S(2)}) collective-permute-start(bf16[3,64,1024]{2,1,0:T(8,128)(2,1)S(1)} %collective-permute-done.2.refs_3_), channel_id=1, source_target_pairs={{0,2},{1,3},{2,4},{3,5},{4,6},{5,7},{6,8},{7,9},{8,10},{9,11},{10,... | collective-permute-start | bytes 1179656 | tf_op jit(solution)/shard_map/ppermute | solution.py:259
  64.7 11.4 %collective-permute-start.5 = (bf16[3,32,1024]{2,1,0:T(8,128)(2,1)S(1)}, bf16[3,32,1024]{2,1,0:T(8,128)(2,1)S(1)}, u32[]{:S(2)}, u32[]{:S(2)}) collective-permute-start(bf16[3,32,1024]{2,1,0:T(8,128)(2,1)S(1)} %slice.9), channel_id=1, source_target_pairs={{0,12},{1,13},{2,14},{3,15},{4,0},{5,1},{6,2},{7,3},{8,4},{9,5},{1... | collective-permute-start | bytes 589832 | tf_op jit(solution)/shard_map/ppermute | solution.py:259
  66.2 16.2 %collective-permute-start.4 = (bf16[3,32,1024]{2,1,0:T(8,128)(2,1)S(1)}, bf16[3,32,1024]{2,1,0:T(8,128)(2,1)S(1)}, u32[]{:S(2)}, u32[]{:S(2)}) collective-permute-start(bf16[3,32,1024]{2,1,0:T(8,128)(2,1)S(1)} %slice.8), channel_id=1, source_target_pairs={{0,4},{1,5},{2,6},{3,7},{4,8},{5,9},{6,10},{7,11},{8,12},{9,13},{1... | collective-permute-start | bytes 589832 | tf_op jit(solution)/shard_map/ppermute | solution.py:259
  76.1 12.8 %collective-permute-start.12 = (bf16[3,64,1024]{2,1,0:T(8,128)(2,1)S(1)}, bf16[3,64,1024]{2,1,0:T(8,128)(2,1)S(1)}, u32[]{:S(2)}, u32[]{:S(2)}) collective-permute-start(bf16[3,64,1024]{2,1,0:T(8,128)(2,1)S(1)} %collective-permute-done.3.refs_4_), channel_id=1, source_target_pairs={{0,1},{1,0},{2,3},{3,2},{4,5},{5,4},{6,7},{7,6},{8,9},{9,8},{10,11... | collective-permute-start | bytes 1179656 | tf_op jit(solution)/shard_map/ppermute | solution.py:263
  88.9 14.9 %collective-permute-start.21 = (bf16[512,512]{1,0:T(8,128)(2,1)S(1)}, bf16[512,512]{1,0:T(8,128)(2,1)S(1)}, u32[]{:S(2)}, u32[]{:S(2)}) collective-permute-start(bf16[512,512]{1,0:T(8,128)(2,1)S(1)} %get-tuple-element.30), channel_id=1, source_target_pairs={{0,128},{16,144},{32,160},{48,176},{64,192},{80,208},{96,224},{112... | collective-permute-start | bytes 1572872 | tf_op jit(solution)/shard_map/ppermute | solution.py:252
  90.7 24.4 %collective-permute-start.22 = (bf16[512,512]{1,0:T(8,128)(2,1)S(1)}, bf16[512,512]{1,0:T(8,128)(2,1)S(1)}, u32[]{:S(2)}, u32[]{:S(2)}) collective-permute-start(bf16[512,512]{1,0:T(8,128)(2,1)S(1)} %get-tuple-element.31), channel_id=1, source_target_pairs={{0,192},{16,208},{32,224},{48,240},{64,0},{80,16},{96,32},{112,48}... | collective-permute-start | bytes 1572872 | tf_op jit(solution)/shard_map/ppermute | solution.py:252
  91.6 23.5 %collective-permute-start.26 = (bf16[512,512]{1,0:T(8,128)(2,1)S(1)}, bf16[512,512]{1,0:T(8,128)(2,1)S(1)}, u32[]{:S(2)}, u32[]{:S(2)}) collective-permute-start(bf16[512,512]{1,0:T(8,128)(2,1)S(1)} %get-tuple-element.34), channel_id=1, source_target_pairs={{0,16},{16,32},{32,48},{48,0},{64,80},{80,96},{96,112},{112,64},{1... | collective-permute-start | bytes 1572872 | tf_op jit(solution)/shard_map/ppermute | solution.py:252
  92.1 24.4 %collective-permute-start.27 = (bf16[512,512]{1,0:T(8,128)(2,1)S(1)}, bf16[512,512]{1,0:T(8,128)(2,1)S(1)}, u32[]{:S(2)}, u32[]{:S(2)}) collective-permute-start(bf16[512,512]{1,0:T(8,128)(2,1)S(1)} %get-tuple-element.35), channel_id=1, source_target_pairs={{0,32},{16,48},{32,0},{48,16},{64,96},{80,112},{96,64},{112,80},{1... | collective-permute-start | bytes 1572872 | tf_op jit(solution)/shard_map/ppermute | solution.py:252
  93.8 23.6 %collective-permute-start.28 = (bf16[512,512]{1,0:T(8,128)(2,1)S(1)}, bf16[512,512]{1,0:T(8,128)(2,1)S(1)}, u32[]{:S(2)}, u32[]{:S(2)}) collective-permute-start(bf16[512,512]{1,0:T(8,128)(2,1)S(1)} %get-tuple-element.36), channel_id=1, source_target_pairs={{0,48},{16,0},{32,16},{48,32},{64,112},{80,64},{96,80},{112,96},{1... | collective-permute-start | bytes 1572872 | tf_op jit(solution)/shard_map/ppermute | solution.py:252
  (18 other events, 166.7 us)
